TPU v7x, 32 devices: a whole 2x2x4 slice. The times are simulated.
32 devices in a mesh: fs: 8 (over z, core), tp: 4 (over y, x).
Axes of the slice: x: 2, y: 2, z: 4, core: 2. Of those that a mesh axis runs over, the one named last changes fastest.
Arguments:
- rows_later: bfloat16 [6144, 2048], P('fs'), may hold values from -6 to 6
- rows_earlier: bfloat16 [6144, 2048], P('fs'), may hold values from -6 to 6
- out_cotangent: bfloat16 [6144, 4096], P('fs', 'tp'), may hold values from -6 to 6
- gate_proj: bfloat16 [2048, 4096], P('fs', 'tp'), may hold values from -0.125 to 0.125
- up_proj: bfloat16 [2048, 4096], P('fs', 'tp'), may hold values from -0.125 to 0.125
- conv_taps: float32 [3, 4096], P(None, 'tp'), may hold values from -4 to 4
- conv_bias: float32 [4096], P('tp'), may hold values from -3 to 3
- gate_grad_sum: float32 [2048, 4096], P('fs', 'tp'), may hold values from -6 to 6
- up_grad_sum: float32 [2048, 4096], P('fs', 'tp'), may hold values from -6 to 6
- taps_grad_sum: float32 [3, 4096], P(None, 'tp'), may hold values from -6 to 6
- bias_grad_sum: float32 [4096], P('tp'), may hold values from -6 to 6
Outputs:
- hidden_later: bfloat16 [6144, 4096], P('fs', 'tp')
- input_grad: bfloat16 [6144, 2048], P('fs')
- gate_grad_out: float32 [2048, 4096], P('fs', 'tp')
- up_grad_out: float32 [2048, 4096], P('fs', 'tp')
- taps_grad_out: float32 [3, 4096], P(None, 'tp')
- bias_grad_out: float32 [4096], P('tp')
All inputs are finite; a program needn't handle non-finite values.
Results may differ from a plain program's by a relative error of at most 0.019.
Values may be sent and summed in bfloat16 or wider, within the bound.
No kernel may reach another device: no remote copies, remote signals or barrier semaphores. Data moves between devices by JAX's collectives and lax.ppermute only.
A program may use at most 128 MiB of HBM per device.

v0:
```python
import jax
import jax.numpy as jnp
from jax import lax
from jax.sharding import PartitionSpec as P


def shift_down(values, distance):
    total_len = values.shape[1]
    return jnp.pad(values, ((0, 0), (distance, 0), (0, 0)))[:, :total_len]


def shift_up(values, distance):
    return jnp.pad(values, ((0, 0), (0, distance), (0, 0)))[:, distance:]


def causal_mix(pre_values, conv_taps, conv_bias):
    return (
        conv_taps[0] * shift_down(pre_values, 2)
        + conv_taps[1] * shift_down(pre_values, 1)
        + conv_taps[2] * pre_values
        + conv_bias
    )


def mix_adjoint(mixed_grad, conv_taps):
    return (
        conv_taps[2] * mixed_grad
        + conv_taps[1] * shift_up(mixed_grad, 1)
        + conv_taps[0] * shift_up(mixed_grad, 2)
    )


def contract_last(left, right):
    return lax.dot_general(
        left, right, (((1,), (1,)), ((), ())), preferred_element_type=jnp.float32
    )


def contract_first(left, right):
    return lax.dot_general(
        left, right, (((0,), (0,)), ((), ())), preferred_element_type=jnp.float32
    )


def on_device(
    rows_later,
    rows_earlier,
    out_cotangent,
    gate_proj,
    up_proj,
    conv_taps,
    conv_bias,
    gate_grad_sum,
    up_grad_sum,
    taps_grad_sum,
    bias_grad_sum,
):
    seq_len = rows_later.shape[0]
    shard_width = out_cotangent.shape[1]
    stacked_rows = jnp.concatenate([rows_later, rows_earlier], axis=0)
    paired = jnp.stack([gate_proj, up_proj], axis=0)
    pieces = lax.all_gather(paired, "fs", axis=1, tiled=True)
    gate_acc = jnp.dot(stacked_rows, pieces[0], preferred_element_type=jnp.float32)
    up_acc = jnp.dot(stacked_rows, pieces[1], preferred_element_type=jnp.float32)
    gate_pre = gate_acc.astype(jnp.bfloat16)
    up_value = up_acc.astype(jnp.bfloat16)
    gate_pre, up_value = lax.optimization_barrier((gate_pre, up_value))
    gate_float = gate_pre.astype(jnp.float32).reshape(2, seq_len, shard_width)
    up_float = up_value.astype(jnp.float32).reshape(2, seq_len, shard_width)
    mixed = causal_mix(gate_float, conv_taps, conv_bias)
    sig_all = jax.nn.sigmoid(mixed)
    activated = mixed * sig_all
    hidden = (activated * up_float).astype(jnp.bfloat16)
    hidden_later = hidden[0]
    grad_scale = lax.rsqrt(jnp.asarray(seq_len * lax.axis_size("fs"), jnp.float32))

    def make_term(grad_rows):
        return contract_first(rows_earlier, grad_rows)

    cotangent = out_cotangent.astype(jnp.float32)[None]
    mixed_back = mixed[1:]
    sig_back = sig_all[1:]
    up_grad = (cotangent * activated[1:]).astype(jnp.bfloat16)[0]
    up_summed = lax.psum_scatter(
        make_term(up_grad).astype(jnp.bfloat16), "fs", scatter_dimension=0, tiled=True
    ).astype(jnp.float32)
    mixed_grad = cotangent * up_float[1:] * sig_back * (1.0 + mixed_back * (1.0 - sig_back))
    gate_grad = mix_adjoint(mixed_grad, conv_taps).astype(jnp.bfloat16)[0]
    gate_summed = lax.psum_scatter(
        make_term(gate_grad).astype(jnp.bfloat16), "fs", scatter_dimension=0, tiled=True
    ).astype(jnp.float32)
    pieces = lax.all_gather(paired, "fs", axis=1, tiled=True)
    partial_rows = contract_last(gate_grad, pieces[0]) + contract_last(up_grad, pieces[1])
    input_grad = lax.psum(partial_rows.astype(jnp.bfloat16), "tp")
    gate_grad_out = gate_grad_sum + grad_scale * gate_summed
    up_grad_out = up_grad_sum + grad_scale * up_summed
    gate_back = gate_float[1:]
    tap_local = jnp.stack(
        [
            jnp.sum(mixed_grad * shift_down(gate_back, 2 - tap_index), axis=(0, 1))
            for tap_index in range(conv_taps.shape[0])
        ]
    )
    bias_local = jnp.sum(mixed_grad, axis=(0, 1))
    tap_total, bias_total = lax.psum((tap_local, bias_local), "fs")
    taps_grad_out = taps_grad_sum + grad_scale * tap_total
    bias_grad_out = bias_grad_sum + grad_scale * bias_total
    return (hidden_later, input_grad, gate_grad_out, up_grad_out, taps_grad_out, bias_grad_out)


def solution(mesh):
    placed = (
        P("fs", None),
        P("fs", None),
        P("fs", "tp"),
        P("fs", "tp"),
        P("fs", "tp"),
        P(None, "tp"),
        P("tp"),
        P("fs", "tp"),
        P("fs", "tp"),
        P(None, "tp"),
        P("tp"),
    )
    return jax.shard_map(
        on_device,
        mesh=mesh,
        in_specs=placed,
        out_specs=(
            P("fs", "tp"),
            P("fs", None),
            P("fs", "tp"),
            P("fs", "tp"),
            P(None, "tp"),
            P("tp"),
        ),
        check_vma=False,
    )
```

profile of v0, /device:TPU:0, one launch (start us, length us, event | category | flops | bytes accessed | tf_op | source)
XLA Modules:
  0.0 333.8 jit_solution(14247439538161545756)
XLA Ops:
  7.2 0.0 copy-start.4
  7.2 0.0 all-gather.2.cloned.1.call-start
  7.2 2.4 pad_maximum_fusion
  9.6 0.0 all-gather.2.cloned.1.call-update
  9.7 0.0 reduce-scatter.3.cloned.1.call-start
  9.7 0.0 copy-start.5
  9.7 0.9 fusion.32
  10.6 0.0 copy-done.4
  10.7 2.0 constant_dynamic-update-slice_fusion.1
  12.6 0.0 copy-done.5
  12.6 2.1 constant_dynamic-update-slice_fusion
  14.8 80.2 %all-gather.2.cloned.1.call-done = bf16[2,2048,1024]{2,1,0:T(8,128)(2,1)} async-done(((bf16[2,256,1024]{2,1,0:T(8,128)(2,1)}), bf16[2,2048,1024]{2,1,0:T(8,128)(2,1)}) %all-gather.2.cloned.1.call-update) | async-done | bytes 8388624 | tf_op jit(solution)/shard_map/all_gather | solution.py:62
  95.0 10.1 %convolution_convert_fusion = bf16[1536,1024]{1,0:T(8,128)(2,1)S(1)} fusion(bf16[1536,2048]{1,0:T(8,128)(2,1)} %constant_dynamic-update-slice_fusion, bf16[2,2048,1024]{2,1,0:T(8,128)(2,1)} %all-gather.2.cloned.1.call-done), kind=kOutput, calls=%fused_computation.15 | convolution fusion | flops 6444023808 | bytes 13631488 | tf_op jit(solution)/shard_map/dot_general | solution.py:64
  105.1 0.0 copy-done.15
  105.1 8.8 %convolution_convert_fusion.1 = bf16[1536,1024]{1,0:T(8,128)(2,1)S(1)} fusion(bf16[1536,2048]{1,0:T(8,128)(2,1)} %constant_dynamic-update-slice_fusion, bf16[2,2048,1024]{2,1,0:T(8,128)(2,1)S(1)} %copy-done.15), kind=kOutput, calls=%fused_computation.16 | convolution fusion | flops 6444023808 | bytes 13631488 | tf_op jit(solution)/shard_map/dot_general | solution.py:63
  113.9 0.7 convert_element_type.59
  114.7 1.9 slice_bitcast_fusion.6
  116.5 0.7 convert_element_type.60
  117.3 0.0 copy-start.1
  117.3 0.0 copy-done.14
  117.3 3.2 add_divide_fusion
  120.5 0.0 copy-start
  120.5 0.6 copy-done.1
  121.1 6.3 %fusion.13 = (f32[1024]{0:T(1024)S(1)}, f32[1024]{0:T(1024)S(1)}, f32[1024]{0:T(1024)S(1)}, f32[1024]{0:T(1024)S(1)}, f32[1,768,1024]{2,1,0:T(8,128)S(1)}) fusion(f32[1,768,1024]{2,1,0:T(8,128)} %slice_bitcast_fusion.6, f32[1536,1024]{1,0:T(8,128)S(1)} %convert_element_type.59, f32[2,768,1024]{2,1,0:T(8,128)S(1)} %get-tuple-element.24, ...), kind=kLoop, calls=%fused_computation.29 | loop fusion | flops 11005952 | bytes 20463616 | tf_op jit(solution)/shard_map/reduce_sum | solution.py:100
  127.4 0.0 copy-done
  127.4 0.0 copy-start.6
  127.4 1.0 fusion.10
  128.4 0.0 copy-start.9
  128.4 1.1 copy-done.9
  129.5 0.0 copy-done.6
  129.5 5.1 %convert_bitcast_fusion.1 = bf16[2048,1024]{0,1:T(8,128)(2,1)} fusion(bf16[768,2048]{1,0:T(8,128)(2,1)S(1)} %copy-done.6, bf16[1,768,1024]{2,1,0:T(8,128)(2,1)S(1)} %fusion.10), kind=kOutput, calls=%fused_computation.12 | convolution fusion | flops 3223322624 | bytes 8912896 | tf_op jit(solution)/shard_map/dot_general | solution.py:40
  134.6 0.0 reduce-scatter.3.cloned.1.call-update
  134.6 0.2 reduce-scatter.5.cloned.1.call-start
  134.9 0.0 copy-start.7
  134.9 4.5 %fusion.29 = f32[2,768,1024]{2,1,0:T(8,128)S(1)} fusion(f32[2,768,1024]{2,1,0:T(8,128)} %copy-done), kind=kLoop, calls=%fused_computation.55 | loop fusion | flops 6291456 | bytes 12582912 | tf_op jit(solution)/shard_map/mul | solution.py:72
  139.4 0.0 copy-start.2
  139.4 2.6 copy-done.2
  142.0 0.0 copy-done.7
  142.0 5.1 %convert_bitcast_fusion = bf16[2048,1024]{0,1:T(8,128)(2,1)} fusion(bf16[768,2048]{1,0:T(8,128)(2,1)S(1)} %copy-done.6, f32[2,768,1024]{2,1,0:T(8,128)S(1)} %fusion.29, bf16[768,1024]{1,0:T(8,128)(2,1)S(1)} %copy-done.7), kind=kOutput, calls=%fused_computation.11 | convolution fusion | flops 3225681920 | bytes 12058624 | tf_op jit(solution)/shard_map/dot_general | solution.py:40
  147.1 0.0 reduce-scatter.5.cloned.1.call-update
  147.2 0.0 copy-start.8
  147.2 0.0 all-reduce.9.cloned.1.call-start
  147.2 1.3 copy-done.10
  148.6 5.5 %fusion.5 = f32[768,2048]{1,0:T(8,128)S(1)} fusion(bf16[2,2048,1024]{2,1,0:T(8,128)(2,1)} %all-gather.2.cloned.1.call-done, bf16[1,768,1024]{2,1,0:T(8,128)(2,1)S(1)} %copy-done.10), kind=kOutput, calls=%fused_computation.17 | convolution fusion | flops 3221225472 | bytes 12058624 | tf_op jit(solution)/shard_map/dot_general | solution.py:34
  154.0 0.0 copy-done.8
  154.0 0.0 copy-done.3
  154.1 0.0 copy-start.11
  154.1 7.3 %add_convert_fusion = bf16[768,2048]{1,0:T(8,128)(2,1)} fusion(f32[768,2048]{1,0:T(8,128)S(1)} %fusion.5, bf16[2,2048,1024]{2,1,0:T(8,128)(2,1)} %all-gather.2.cloned.1.call-done, f32[2,768,1024]{2,1,0:T(8,128)S(1)} %copy-done.3, bf16[768,1024]{1,0:T(8,128)(2,1)S(1)} %copy-done.8), kind=kOutput, calls=%fused_computation.7 | convolution fusion | flops 3226730496 | bytes 18350080 | tf_op jit(solution)/shard_map/dot_general | solution.py:34
  161.4 0.0 all-reduce.9.cloned.1.call-update
  161.4 0.0 copy-done.11
  161.4 0.3 copy.17
  161.8 1.6 copy.18
  163.4 27.1 %all-reduce.6 = (f32[3,1024]{1,0:T(4,128)S(1)}, f32[1024]{0:T(1024)S(1)}) all-reduce(f32[3,1024]{1,0:T(4,128)S(1)} %pad_maximum_fusion.1, f32[1024]{0:T(1024)S(1)} %get-tuple-element.18), channel_id=1, replica_groups=mesh['fs'=8,'tp'=4] {'fs'}, use_global_device_ids=true, to_apply=%region_6.7 | all-reduce | flops 4096 | bytes 32768 | tf_op jit(solution)/shard_map/psum | solution.py:105
  190.5 0.0 copy-done.13
  190.5 0.6 multiply_add_fusion.3
  191.1 0.6 multiply_add_fusion.2
  191.7 4.5 %fusion.23 = bf16[768,1024]{1,0:T(8,128)(2,1)} fusion(f32[2,768,1024]{2,1,0:T(8,128)} %bitcast.61, f32[2,768,1024]{2,1,0:T(8,128)} %copy-done.2), kind=kLoop, calls=%fused_computation.43 | loop fusion | flops 1572864 | bytes 7864320 | tf_op jit(solution)/shard_map/squeeze | solution.py:74
  196.2 1.2 multiply_add_fusion.1
  197.4 1.3 copy.19
  198.7 35.6 %reduce-scatter.5.cloned.1.call-done = bf16[256,1024]{0,1:T(8,128)(2,1)} async-done(((bf16[2048,1024]{0,1:T(8,128)(2,1)}), bf16[256,1024]{0,1:T(8,128)(2,1)}) %reduce-scatter.5.cloned.1.call-update) | async-done | bytes 524304 | tf_op jit(solution)/shard_map/reduce_scatter | solution.py:84
  234.3 1.2 multiply_add_fusion
  235.5 1.3 copy.20
  236.8 86.5 %all-reduce.9.cloned.1.call-done = bf16[768,2048]{1,0:T(8,128)(2,1)} async-done(((bf16[768,2048]{1,0:T(8,128)(2,1)}), bf16[768,2048]{1,0:T(8,128)(2,1)}) %all-reduce.9.cloned.1.call-update) | async-done | bytes 3145744 | tf_op jit(solution)/shard_map/psum | solution.py:94
  323.3 4.0 %copy.23 = bf16[768,2048]{1,0:T(8,128)(2,1)} copy(bf16[768,2048]{1,0:T(8,128)(2,1)} %all-reduce.9.cloned.1.call-done) | data formatting | bytes 6291456
  (9 shorter events, 0.0 us)
Async XLA Ops:
  7.2 3.5 %copy-start.4 = (bf16[768,2048]{1,0:T(8,128)(2,1)S(1)}, bf16[768,2048]{1,0:T(8,128)(2,1)}, u32[]{:S(2)}) copy-start(bf16[768,2048]{1,0:T(8,128)(2,1)} %param.11) | copy-start | bytes 9437188
  7.2 87.8 %all-gather.2.cloned.1.call-start = ((), (), s32[]{:S(2)}) async-start(), calls=%async_computation.2 | async-start | bytes 9437184 | tf_op jit(solution)/shard_map/all_gather | solution.py:62
  9.7 186.6 %reduce-scatter.3.cloned.1.call-start = ((), (), s32[]{:S(2)}) async-start(), calls=%async_computation.4 | async-start | bytes 4718592 | tf_op jit(solution)/shard_map/reduce_scatter | solution.py:89
  9.7 2.9 copy-start.5
  95.0 10.1 %copy-start.15 = (bf16[2,2048,1024]{2,1,0:T(8,128)(2,1)S(1)}, bf16[2,2048,1024]{2,1,0:T(8,128)(2,1)}, u32[]{:S(2)}) copy-start(bf16[2,2048,1024]{2,1,0:T(8,128)(2,1)} %all-gather.2.cloned.1.call-done) | copy-start | bytes 25165828
  116.5 0.7 copy-start.14
  117.3 3.8 %copy-start.1 = (f32[1536,1024]{1,0:T(8,128)}, f32[1536,1024]{1,0:T(8,128)S(1)}, u32[]{:S(2)}) copy-start(f32[1536,1024]{1,0:T(8,128)S(1)} %convert_element_type.60) | copy-start | bytes 18874372
  120.5 6.9 %copy-start = (f32[2,768,1024]{2,1,0:T(8,128)}, f32[2,768,1024]{2,1,0:T(8,128)S(1)}, u32[]{:S(2)}) copy-start(f32[2,768,1024]{2,1,0:T(8,128)S(1)} %get-tuple-element.24) | copy-start | bytes 18874372
  127.4 2.2 copy-start.6
  128.4 1.1 copy-start.9
  134.6 99.7 %reduce-scatter.5.cloned.1.call-start = ((), (), s32[]{:S(2)}) async-start(), calls=%async_computation.5 | async-start | bytes 4718592 | tf_op jit(solution)/shard_map/reduce_scatter | solution.py:84
  134.9 7.1 %copy-start.7 = (bf16[768,1024]{1,0:T(8,128)(2,1)S(1)}, bf16[768,1024]{1,0:T(8,128)(2,1)}, u32[]{:S(2)}) copy-start(bf16[768,1024]{1,0:T(8,128)(2,1)} %param.13) | copy-start | bytes 4718596
  139.4 2.6 copy-start.2
  147.1 1.4 copy-start.10
  147.2 6.9 %copy-start.8 = (bf16[768,1024]{1,0:T(8,128)(2,1)S(1)}, bf16[768,1024]{1,0:T(8,128)(2,1)}, u32[]{:S(2)}) copy-start(bf16[768,1024]{1,0:T(8,128)(2,1)} %param.13) | copy-start | bytes 4718596
  147.2 176.1 %all-reduce.9.cloned.1.call-start = ((), (), s32[]{:S(2)}) async-start(), calls=%async_computation.3 | async-start | bytes 6291456 | tf_op jit(solution)/shard_map/psum | solution.py:94
  148.6 5.5 %copy-start.3 = (f32[2,768,1024]{2,1,0:T(8,128)S(1)}, f32[2,768,1024]{2,1,0:T(8,128)}, u32[]{:S(2)}) copy-start(f32[2,768,1024]{2,1,0:T(8,128)} %copy-done.2) | copy-start | bytes 18874372
  154.1 7.4 %copy-start.11 = (f32[256,1024]{1,0:T(8,128)S(1)}, f32[256,1024]{1,0:T(8,128)}, u32[]{:S(2)}) copy-start(f32[256,1024]{1,0:T(8,128)} %param.18) | copy-start | bytes 3145732
  161.4 29.1 %copy-start.13 = (f32[1024]{0:T(1024)S(1)}, f32[1024]{0:T(1024)}, u32[]{:S(2)}) copy-start(f32[1024]{0:T(1024)} %param.21) | copy-start | bytes 12292
  161.4 29.7 %copy-start.12 = (f32[3,1024]{1,0:T(4,128)S(1)}, f32[3,1024]{1,0:T(4,128)}, u32[]{:S(2)}) copy-start(f32[3,1024]{1,0:T(4,128)} %param.20) | copy-start | bytes 36868
Sparse Core Ops, SparseCore 0:
  10.2 84.7 all-gather.1
  134.8 48.8 reduce-scatter.2
  185.9 48.3 reduce-scatter.4
  237.9 85.4 all-reduce.8
where the time goes:
time: 334 us
  waiting for transfers between devices  202 us (60%)
  matrix products  42 us (13%)
  blocking collectives  27.1 us (8%)
  other arithmetic  26.9 us (8%)
  local copies, waits for them, and re-layouts  21.1 us (6%)
  between operations  14 us (4%)
    psum x1, waiting for transfers between devices, on_device(): input_grad = lax.psum(partial_rows.astype(jnp.bfloat16), 'tp')  86.5 us
    all_gather x1, waiting for transfers between devices, on_device(): pieces = lax.all_gather(paired, 'fs', axis=1, tiled=True)  80.2 us
    reduce_scatter x1, waiting for transfers between devices, on_device(): lax.psum_scatter(make_term(up_grad).astype(jnp.bfloat16), 'fs', scatter_d...  35.6 us
    psum x1, blocking collectives, on_device(): tap_total, bias_total = lax.psum((tap_local, bias_local), 'fs')  27.1 us
    unnamed x38, local copies, waits for them, and re-layouts  16.1 us
    dot_general x2, matrix products, contract_last(): lax.dot_general(left, right, (((1,), (1,)), ((), ())), preferred_element_...  12.8 us
    dot_general x2, matrix products, contract_first(): lax.dot_general(left, right, (((0,), (0,)), ((), ())), preferred_element_...  10.2 us
    dot_general x1, matrix products, on_device(): jnp.dot(stacked_rows, pieces[1], preferred_element_type=jnp.float32)  10.1 us
  transfers between devices with their start and end apart: 4, of which 3 were waited for; matrix products, arithmetic and copies ran while one was open for 12% of the time, Pallas kernels for 0%

commit v1 on v0

--- a/solution.py
+++ b/solution.py
@@ -91,7 +91,8 @@
     ).astype(jnp.float32)
     pieces = lax.all_gather(paired, "fs", axis=1, tiled=True)
     partial_rows = contract_last(gate_grad, pieces[0]) + contract_last(up_grad, pieces[1])
-    input_grad = lax.psum(partial_rows.astype(jnp.bfloat16), "tp")
+    here_x = partial_rows.astype(jnp.bfloat16)
+    input_grad = jnp.sum(lax.all_gather(here_x, axis_name="tp"), axis=0)
     gate_grad_out = gate_grad_sum + grad_scale * gate_summed
     up_grad_out = up_grad_sum + grad_scale * up_summed
     gate_back = gate_float[1:]

time: 334 us -> 375 us (1.12)
  waiting for transfers between devices: 202 us -> 237 us
  other arithmetic: 26.9 us -> 37.2 us
  local copies, waits for them, and re-layouts: 21.1 us -> 17.1 us
    all_gather x0 -> x1, waiting for transfers between devices: none -> 121 us  [on_device(): input_grad = jnp.sum(lax.all_gather(here_x, axis_name='tp'), axis=0)]
    psum x1 -> x0, waiting for transfers between devices: 86.5 us -> none  [on_device(): input_grad = lax.psum(partial_rows.astype(jnp.bfloat16), 'tp')]
    reduce_sum x0 -> x1, other arithmetic: none -> 10.3 us  [on_device(): input_grad = jnp.sum(lax.all_gather(here_x, axis_name='tp'), axis=0)]
    unnamed x38 -> x37, local copies, waits for them, and re-layouts: 16.1 us -> 12.2 us
  transfers between devices with their start and end apart: 4 -> 4, of which waited for: 3 -> 3; matrix products, arithmetic and copies ran while one was open for 12% -> 11% of each run, Pallas kernels for 0% -> 0%
where the time goes in v1:
time: 375 us; the launch traced here: 374 us
  waiting for transfers between devices  237 us (63%)
  matrix products  42 us (11%)
  other arithmetic  37.2 us (10%)
  blocking collectives  27.1 us (7%)
  local copies, waits for them, and re-layouts  17.1 us (5%)
  between operations  14 us (4%)
    all_gather x1, waiting for transfers between devices, on_device(): input_grad = jnp.sum(lax.all_gather(here_x, axis_name='tp'), axis=0)  121 us
    all_gather x1, waiting for transfers between devices, on_device(): pieces = lax.all_gather(paired, 'fs', axis=1, tiled=True)  80.2 us
    reduce_scatter x1, waiting for transfers between devices, on_device(): lax.psum_scatter(make_term(up_grad).astype(jnp.bfloat16), 'fs', scatter_d...  35.6 us
    psum x1, blocking collectives, on_device(): tap_total, bias_total = lax.psum((tap_local, bias_local), 'fs')  27.1 us
    dot_general x2, matrix products, contract_last(): lax.dot_general(left, right, (((1,), (1,)), ((), ())), preferred_element_...  12.8 us
    unnamed x37, local copies, waits for them, and re-layouts  12.2 us
    reduce_sum x1, other arithmetic, on_device(): input_grad = jnp.sum(lax.all_gather(here_x, axis_name='tp'), axis=0)  10.3 us
    dot_general x2, matrix products, contract_first(): lax.dot_general(left, right, (((0,), (0,)), ((), ())), preferred_element_...  10.2 us
  transfers between devices with their start and end apart: 4, of which 3 were waited for; matrix products, arithmetic and copies ran while one was open for 11% of the time, Pallas kernels for 0%

profile of v1, /device:TPU:0, one launch (start us, length us, event | category | flops | bytes accessed | tf_op | source)
XLA Modules:
  0.0 374.4 jit_solution(15005811123654166943)
XLA Ops:
  7.2 0.0 copy-start.4
  7.2 0.0 all-gather.4.cloned.1.call-start
  7.2 2.4 pad_maximum_fusion
  9.6 0.0 all-gather.4.cloned.1.call-update
  9.7 0.0 reduce-scatter.3.cloned.1.call-start
  9.7 0.0 copy-start.5
  9.7 0.9 fusion.32
  10.6 0.0 copy-done.4
  10.7 2.0 constant_dynamic-update-slice_fusion.1
  12.6 0.0 copy-done.5
  12.6 2.1 constant_dynamic-update-slice_fusion
  14.8 80.2 %all-gather.4.cloned.1.call-done = bf16[2,2048,1024]{2,1,0:T(8,128)(2,1)} async-done(((bf16[2,256,1024]{2,1,0:T(8,128)(2,1)}), bf16[2,2048,1024]{2,1,0:T(8,128)(2,1)}) %all-gather.4.cloned.1.call-update) | async-done | bytes 8388624 | tf_op jit(solution)/shard_map/all_gather | solution.py:62
  95.0 10.1 %convolution_convert_fusion = bf16[1536,1024]{1,0:T(8,128)(2,1)S(1)} fusion(bf16[1536,2048]{1,0:T(8,128)(2,1)} %constant_dynamic-update-slice_fusion, bf16[2,2048,1024]{2,1,0:T(8,128)(2,1)} %all-gather.4.cloned.1.call-done), kind=kOutput, calls=%fused_computation.15 | convolution fusion | flops 6444023808 | bytes 13631488 | tf_op jit(solution)/shard_map/dot_general | solution.py:64
  105.1 0.0 copy-done.15
  105.1 8.8 %convolution_convert_fusion.1 = bf16[1536,1024]{1,0:T(8,128)(2,1)S(1)} fusion(bf16[1536,2048]{1,0:T(8,128)(2,1)} %constant_dynamic-update-slice_fusion, bf16[2,2048,1024]{2,1,0:T(8,128)(2,1)S(1)} %copy-done.15), kind=kOutput, calls=%fused_computation.16 | convolution fusion | flops 6444023808 | bytes 13631488 | tf_op jit(solution)/shard_map/dot_general | solution.py:63
  113.9 0.7 convert_element_type.61
  114.7 1.9 slice_bitcast_fusion.6
  116.5 0.7 convert_element_type.62
  117.3 0.0 copy-start.1
  117.3 0.0 copy-done.14
  117.3 3.2 add_divide_fusion
  120.5 0.0 copy-start
  120.5 0.6 copy-done.1
  121.1 6.3 %fusion.13 = (f32[1024]{0:T(1024)S(1)}, f32[1024]{0:T(1024)S(1)}, f32[1024]{0:T(1024)S(1)}, f32[1024]{0:T(1024)S(1)}, f32[1,768,1024]{2,1,0:T(8,128)S(1)}) fusion(f32[1,768,1024]{2,1,0:T(8,128)} %slice_bitcast_fusion.6, f32[1536,1024]{1,0:T(8,128)S(1)} %convert_element_type.61, f32[2,768,1024]{2,1,0:T(8,128)S(1)} %get-tuple-element.24, ...), kind=kLoop, calls=%fused_computation.29 | loop fusion | flops 11005952 | bytes 20463616 | tf_op jit(solution)/shard_map/reduce_sum | solution.py:101
  127.4 0.0 copy-done
  127.4 0.0 copy-start.6
  127.4 1.0 fusion.10
  128.4 0.0 copy-start.9
  128.4 1.1 copy-done.9
  129.5 0.0 copy-done.6
  129.5 5.1 %convert_bitcast_fusion.1 = bf16[2048,1024]{0,1:T(8,128)(2,1)} fusion(bf16[768,2048]{1,0:T(8,128)(2,1)S(1)} %copy-done.6, bf16[1,768,1024]{2,1,0:T(8,128)(2,1)S(1)} %fusion.10), kind=kOutput, calls=%fused_computation.12 | convolution fusion | flops 3223322624 | bytes 8912896 | tf_op jit(solution)/shard_map/dot_general | solution.py:40
  134.7 0.0 reduce-scatter.3.cloned.1.call-update
  134.7 0.2 reduce-scatter.5.cloned.1.call-start
  134.9 0.0 copy-start.7
  134.9 4.5 %fusion.29 = f32[2,768,1024]{2,1,0:T(8,128)S(1)} fusion(f32[2,768,1024]{2,1,0:T(8,128)} %copy-done), kind=kLoop, calls=%fused_computation.55 | loop fusion | flops 6291456 | bytes 12582912 | tf_op jit(solution)/shard_map/mul | solution.py:72
  139.5 0.0 copy-start.2
  139.5 2.6 copy-done.2
  142.1 0.0 copy-done.7
  142.1 5.1 %convert_bitcast_fusion = bf16[2048,1024]{0,1:T(8,128)(2,1)} fusion(bf16[768,2048]{1,0:T(8,128)(2,1)S(1)} %copy-done.6, f32[2,768,1024]{2,1,0:T(8,128)S(1)} %fusion.29, bf16[768,1024]{1,0:T(8,128)(2,1)S(1)} %copy-done.7), kind=kOutput, calls=%fused_computation.11 | convolution fusion | flops 3225681920 | bytes 12058624 | tf_op jit(solution)/shard_map/dot_general | solution.py:40
  147.2 0.0 reduce-scatter.5.cloned.1.call-update
  147.2 0.0 copy-start.8
  147.2 0.0 all-gather.6.cloned.1.call-start
  147.3 1.3 copy-done.10
  148.6 5.5 %fusion.5 = f32[768,2048]{1,0:T(8,128)S(1)} fusion(bf16[2,2048,1024]{2,1,0:T(8,128)(2,1)} %all-gather.4.cloned.1.call-done, bf16[1,768,1024]{2,1,0:T(8,128)(2,1)S(1)} %copy-done.10), kind=kOutput, calls=%fused_computation.17 | convolution fusion | flops 3221225472 | bytes 12058624 | tf_op jit(solution)/shard_map/dot_general | solution.py:34
  154.1 0.0 copy-done.8
  154.1 0.0 copy-done.3
  154.1 0.0 copy-start.11
  154.1 7.3 %add_convert_fusion = bf16[768,2048]{1,0:T(8,128)(2,1)} fusion(f32[768,2048]{1,0:T(8,128)S(1)} %fusion.5, bf16[2,2048,1024]{2,1,0:T(8,128)(2,1)} %all-gather.4.cloned.1.call-done, f32[2,768,1024]{2,1,0:T(8,128)S(1)} %copy-done.3, bf16[768,1024]{1,0:T(8,128)(2,1)S(1)} %copy-done.8), kind=kOutput, calls=%fused_computation.7 | convolution fusion | flops 3226730496 | bytes 18350080 | tf_op jit(solution)/shard_map/dot_general | solution.py:34
  161.5 0.0 all-gather.6.cloned.1.call-update
  161.5 0.0 copy-done.11
  161.5 0.3 copy.17
  161.8 1.6 copy.18
  163.4 27.1 %all-reduce.6 = (f32[3,1024]{1,0:T(4,128)S(1)}, f32[1024]{0:T(1024)S(1)}) all-reduce(f32[3,1024]{1,0:T(4,128)S(1)} %pad_maximum_fusion.1, f32[1024]{0:T(1024)S(1)} %get-tuple-element.18), channel_id=1, replica_groups=mesh['fs'=8,'tp'=4] {'fs'}, use_global_device_ids=true, to_apply=%region_6.7 | all-reduce | flops 4096 | bytes 32768 | tf_op jit(solution)/shard_map/psum | solution.py:106
  190.6 0.6 multiply_add_fusion.3
  191.2 0.0 copy-done.12
  191.2 0.6 multiply_add_fusion.2
  191.8 4.5 %fusion.23 = bf16[768,1024]{1,0:T(8,128)(2,1)} fusion(f32[2,768,1024]{2,1,0:T(8,128)} %bitcast.62, f32[2,768,1024]{2,1,0:T(8,128)} %copy-done.2), kind=kLoop, calls=%fused_computation.43 | loop fusion | flops 1572864 | bytes 7864320 | tf_op jit(solution)/shard_map/squeeze | solution.py:74
  196.3 1.2 multiply_add_fusion.1
  197.5 1.3 copy.19
  198.8 35.6 %reduce-scatter.5.cloned.1.call-done = bf16[256,1024]{0,1:T(8,128)(2,1)} async-done(((bf16[2048,1024]{0,1:T(8,128)(2,1)}), bf16[256,1024]{0,1:T(8,128)(2,1)}) %reduce-scatter.5.cloned.1.call-update) | async-done | bytes 524304 | tf_op jit(solution)/shard_map/reduce_scatter | solution.py:84
  234.4 1.2 multiply_add_fusion
  235.6 1.3 copy.20
  236.9 120.7 %all-gather.6.cloned.1.call-done = bf16[3072,2048]{1,0:T(8,128)(2,1)} async-done(((bf16[768,2048]{1,0:T(8,128)(2,1)}), bf16[3072,2048]{1,0:T(8,128)(2,1)}) %all-gather.6.cloned.1.call-update) | async-done | bytes 12582928 | tf_op jit(solution)/shard_map/all_gather | solution.py:95
  357.5 10.3 %reduce_sum.48 = bf16[768,2048]{1,0:T(8,128)(2,1)} reduce(bf16[4,768,2048]{2,1,0:T(8,128)(2,1)} %bitcast.63, bf16[]{:T(256)} %constant.6.clone.1), dimensions={0}, to_apply=%region_0.1 | reduce | flops 4718592 | bytes 15728642 | tf_op jit(solution)/shard_map/reduce_sum | solution.py:95
  (9 shorter events, 0.0 us)
Async XLA Ops:
  7.2 3.5 copy-start.4
  7.2 87.8 %all-gather.4.cloned.1.call-start = ((), (), s32[]{:S(2)}) async-start(), calls=%async_computation.2 | async-start | bytes 9437184 | tf_op jit(solution)/shard_map/all_gather | solution.py:62
  9.7 186.6 %reduce-scatter.3.cloned.1.call-start = ((), (), s32[]{:S(2)}) async-start(), calls=%async_computation.3 | async-start | bytes 4718592 | tf_op jit(solution)/shard_map/reduce_scatter | solution.py:89
  9.7 2.9 copy-start.5
  95.0 10.1 %copy-start.15 = (bf16[2,2048,1024]{2,1,0:T(8,128)(2,1)S(1)}, bf16[2,2048,1024]{2,1,0:T(8,128)(2,1)}, u32[]{:S(2)}) copy-start(bf16[2,2048,1024]{2,1,0:T(8,128)(2,1)} %all-gather.4.cloned.1.call-done) | copy-start | bytes 25165828
  116.5 0.7 copy-start.14
  117.3 3.8 %copy-start.1 = (f32[1536,1024]{1,0:T(8,128)}, f32[1536,1024]{1,0:T(8,128)S(1)}, u32[]{:S(2)}) copy-start(f32[1536,1024]{1,0:T(8,128)S(1)} %convert_element_type.62) | copy-start | bytes 18874372
  120.5 6.9 %copy-start = (f32[2,768,1024]{2,1,0:T(8,128)}, f32[2,768,1024]{2,1,0:T(8,128)S(1)}, u32[]{:S(2)}) copy-start(f32[2,768,1024]{2,1,0:T(8,128)S(1)} %get-tuple-element.24) | copy-start | bytes 18874372
  127.4 2.2 copy-start.6
  128.4 1.1 copy-start.9
  134.7 99.7 %reduce-scatter.5.cloned.1.call-start = ((), (), s32[]{:S(2)}) async-start(), calls=%async_computation.4 | async-start | bytes 4718592 | tf_op jit(solution)/shard_map/reduce_scatter | solution.py:84
  134.9 7.2 %copy-start.7 = (bf16[768,1024]{1,0:T(8,128)(2,1)S(1)}, bf16[768,1024]{1,0:T(8,128)(2,1)}, u32[]{:S(2)}) copy-start(bf16[768,1024]{1,0:T(8,128)(2,1)} %param.13) | copy-start | bytes 4718596
  139.5 2.6 copy-start.2
  147.2 1.4 copy-start.10
  147.2 6.9 %copy-start.8 = (bf16[768,1024]{1,0:T(8,128)(2,1)S(1)}, bf16[768,1024]{1,0:T(8,128)(2,1)}, u32[]{:S(2)}) copy-start(bf16[768,1024]{1,0:T(8,128)(2,1)} %param.13) | copy-start | bytes 4718596
  147.2 210.3 %all-gather.6.cloned.1.call-start = ((), (), s32[]{:S(2)}) async-start(), calls=%async_computation.5 | async-start | bytes 15728640 | tf_op jit(solution)/shard_map/all_gather | solution.py:95
  148.6 5.5 %copy-start.3 = (f32[2,768,1024]{2,1,0:T(8,128)S(1)}, f32[2,768,1024]{2,1,0:T(8,128)}, u32[]{:S(2)}) copy-start(f32[2,768,1024]{2,1,0:T(8,128)} %copy-done.2) | copy-start | bytes 18874372
  154.1 7.4 %copy-start.11 = (f32[256,1024]{1,0:T(8,128)S(1)}, f32[256,1024]{1,0:T(8,128)}, u32[]{:S(2)}) copy-start(f32[256,1024]{1,0:T(8,128)} %param.18) | copy-start | bytes 3145732
  161.5 29.1 %copy-start.13 = (f32[1024]{0:T(1024)S(1)}, f32[1024]{0:T(1024)}, u32[]{:S(2)}) copy-start(f32[1024]{0:T(1024)} %param.21) | copy-start | bytes 12292
  161.5 29.7 %copy-start.12 = (f32[3,1024]{1,0:T(4,128)S(1)}, f32[3,1024]{1,0:T(4,128)}, u32[]{:S(2)}) copy-start(f32[3,1024]{1,0:T(4,128)} %param.20) | copy-start | bytes 36868
Sparse Core Ops, SparseCore 0:
  10.2 84.7 all-gather.3
  134.8 48.8 reduce-scatter.2
  186.0 48.3 reduce-scatter.4
  236.7 120.8 all-gather.5
